TPU v7x, 512 devices: a whole 4x8x8 slice. The times are simulated.
512 devices in a mesh: ep: 128 (over z, y, core), tp: 4 (over x).
Axes of the slice: x: 4, y: 8, z: 8, core: 2. Of those that a mesh axis runs over, the one named last changes fastest.
Arguments:
- tokens: bfloat16 [384, 2048], P('ep'), may hold values from -6 to 6
- mixer_gain: float32 [2048], replicated, may hold values from 0.1 to 1.9
- query_weight: bfloat16 [2048, 2048], P('ep', 'tp'), may hold values from -0.125 to 0.125
- key_cache: bfloat16 [384, 1024, 4, 128], P('ep', None, 'tp'), may hold values from -6 to 6
- value_cache: bfloat16 [384, 1024, 4, 128], P('ep', None, 'tp'), may hold values from -6 to 6
- seq_lengths: int32 [384], P('ep'), may hold values from 1 to 1024, as said below
- head_offset: float32 [16], P('tp'), may hold values from -8.5 to -3.5
- output_weight: bfloat16 [2048, 2048], P('tp', 'ep'), may hold values from -0.5 to 0.5
- expert_gain: float32 [2048], replicated, may hold values from 0.1 to 1.9
- expert_ids: int32 [384, 2], P('ep'), may hold values from 0 to 127, as said below
- route_weight: float32 [384, 2], P('ep'), may hold values from 0.2 to 1
- gate_weight: bfloat16 [128, 2048, 1024], P('ep', None, 'tp'), may hold values from -0.125 to 0.125
- up_weight: bfloat16 [128, 2048, 1024], P('ep', None, 'tp'), may hold values from -0.125 to 0.125
- down_weight: bfloat16 [128, 1024, 2048], P('ep', 'tp'), may hold values from -0.1875 to 0.1875
Outputs:
- layer_out: bfloat16 [384, 2048], P('ep', 'tp')
Inputs may be any that keep to these rules, and one draw needn't show every extreme that they name: `seq_lengths`: some sequence holds all 1024 positions. `expert_ids`: the 2 experts of a row are different and lie in one group of 4 consecutive expert numbers. Among the 3 rows of one index of ep no expert is named by more than 2 rows, and some expert by exactly 2.
All inputs are finite; a program needn't handle non-finite values.
Results may differ from a plain program's by a relative error of at most 0.012.
Values may be sent and summed in bfloat16 or wider, within the bound.
A program may use at most 64 MiB of HBM per device.

v0:
```python
import functools
from types import SimpleNamespace

import jax
import jax.numpy as jnp
from jax import lax
from jax.experimental import pallas as pl
from jax.experimental.pallas import tpu as pltpu
from jax.sharding import Mesh
from jax.sharding import PartitionSpec as P

EP = ("z", "y", "c")
SLOTS = 16
PAD = 4
F32 = jnp.float32
BF16 = jnp.bfloat16


def iota(shape, dim):
    return lax.broadcasted_iota(jnp.int32, shape, dim)


def dot(a, b, dims=((1,), (0,)), precision=None):
    return lax.dot_general(a, b, (dims, ((), ())), precision=precision, preferred_element_type=F32)


def onehot(condition):
    return jnp.where(condition, 1.0, 0.0).astype(BF16)


def near_first(count):
    return sorted(range(1, count), key=lambda k: min(k, count - k))


def far_first(count):
    return near_first(count)[::-1]


def stacked(ref, count):
    return jnp.concatenate([ref[t].astype(F32) for t in range(count)], axis=0).astype(BF16)


def remote(src, dst, send_sem, recv_sem, **where):
    return pltpu.make_async_remote_copy(
        src_ref=src,
        dst_ref=dst,
        send_sem=send_sem,
        recv_sem=recv_sem,
        device_id=where,
        device_id_type=pl.DeviceIdType.MESH,
    )


def attention(d, q, kbuf, vbuf, lens, hoff):
    heads = d.ql // d.hd
    rows = heads * 8
    queries = jnp.concatenate([q[:, h * d.hd : (h + 1) * d.hd] for h in range(heads)], axis=0)
    queries = queries.astype(BF16)
    row = iota((rows, 1), 0)
    seq = row & 7
    head = row >> 3
    score = jnp.zeros((rows, d.cache), F32)
    length = jnp.zeros((rows, 1), jnp.int32)
    offset = jnp.zeros((rows, 1), F32)
    for b in range(d.b):
        one = dot(queries, kbuf[b], ((1,), (1,)))
        score = jnp.where(seq == b, one, score)
        length = jnp.where(seq == b, lens[b], length)
    for h in range(heads):
        offset = jnp.where(head == h, hoff[h], offset)
    score = score * (d.hd**-0.5) + offset
    valid = iota((rows, d.cache), 1) < length
    soft = jnp.log1p(jnp.exp(-jnp.abs(score)))
    log_take = jnp.minimum(score, 0.0) - soft
    log_pass = jnp.where(valid, jnp.minimum(-score, 0.0) - soft, 0.0)
    blocks = d.cache // 128
    pieces = [log_pass[:, i * 128 : (i + 1) * 128] for i in range(blocks)]
    after = (iota((128, 128), 0) > iota((128, 128), 1)).astype(F32)
    inside = dot(jnp.concatenate(pieces, axis=0), after, precision=lax.Precision.HIGHEST)
    later = jnp.zeros((rows, 1), F32)
    sums = [None] * blocks
    for i in range(blocks - 1, -1, -1):
        sums[i] = inside[i * rows : (i + 1) * rows] + later
        later = later + jnp.sum(pieces[i], axis=1, keepdims=True)
    weight = jnp.where(valid, jnp.exp(log_take + jnp.concatenate(sums, axis=1)), 0.0).astype(BF16)
    total = jnp.zeros((rows, d.hd), F32)
    for b in range(d.b):
        total = jnp.where(seq == b, dot(weight, vbuf[b]), total)
    return jnp.concatenate([total[h * 8 : (h + 1) * 8] for h in range(heads)], axis=1).astype(BF16)


def kernel(d, *refs):
    (tokens_in, mgain_in, wq_in_hbm, key, val, lens_in, hoff_in, wo_in_hbm, egain_in, ids_in, rw_in,
     gate, up, down) = refs[:14]
    out, line_out, info_out, most_out = refs[14:18]
    (tokens, mgain, wq, wo, egain, lens, hoff, ids, rw,
     kbuf, vbuf, gbuf, ubuf, dbuf, load_sem,
     ta_send, ta_recv, qa_send, qa_recv, wq_all, wo_all, qp_send, qp_recv, mx_send, mx_recv,
     pt_send, pt_recv, rb_send, line_rows, own_send, rows, s_send, s_recv, h_send, h_recv,
     y_send, y_recv, z_send, z_recv,
     info_a, info_az, info_b, info_by, info_c, info_cc,
     zs, zr, ys, yr, xs, xr, cs, cr) = refs[18:]
    z, y, c, x = (lax.axis_index(name) for name in ("z", "y", "c", "x"))
    nz, ny, nc, nx, b = d.nz, d.ny, d.nc, d.nx, d.b
    other = 1 - c
    slot = c * ny + y
    line = nz * b
    home = z // d.nb
    MESH = pl.DeviceIdType.MESH

    def up_z(k):
        return lax.rem(z + k, nz)

    def up_y(k):
        return lax.rem(y + k, ny)

    def up_x(k):
        return lax.rem(x + k, nx)

    def up_c(k):
        return lax.rem(c + k, nc)

    small = [
        pltpu.make_async_copy(src, dst, load_sem.at[14 + i])
        for i, (src, dst) in enumerate([
            (tokens_in, tokens), (mgain_in, mgain), (wq_in_hbm, wq), (ids_in, ids), (rw_in, rw),
            (wo_in_hbm, wo), (lens_in, lens), (hoff_in, hoff), (egain_in, egain),
        ])
    ]
    for copy in small:
        copy.start()
    barrier = pltpu.get_barrier_semaphore()
    peers = [{"z": up_z(k), "c": up_c(j)} for k in far_first(nz) for j in range(nc)]
    peers += [{"y": up_y(k)} for k in far_first(ny)]
    peers += [{"x": up_x(k), "c": up_c(j)} for k in far_first(nx) for j in range(nc)]
    peers += [{"c": other}]
    for peer in peers:
        pl.semaphore_signal(barrier, inc=1, device_id=peer, device_id_type=MESH)

    loads = [
        pltpu.make_async_copy(src, dst, load_sem.at[i])
        for i, (src, dst) in enumerate(
            [(key, kbuf), (val, vbuf), (gate, gbuf), (up, ubuf), (down, dbuf)]
        )
    ]
    for copy in loads:
        copy.start()
    for copy in small:
        copy.wait()

    wide = tokens[...].astype(F32)
    scale = lax.rsqrt(jnp.mean(wide * wide, axis=1, keepdims=True) + 1e-06)
    normed = (wide * scale * mgain[...]).astype(BF16).astype(F32)
    filler = jnp.zeros((PAD - b, d.width), F32)
    normed = jnp.concatenate([normed, filler], axis=0)
    plain = jnp.concatenate([wide, filler], axis=0).astype(BF16)
    for t in range(nz):
        ta_send[t] = plain[:, t * d.zb : (t + 1) * d.zb]
    share = ny * d.rp
    depth, tall = d.rp.bit_length() - 1, share.bit_length() - 1
    to = iota((d.zb, d.zb), 1)
    source = ((((to & (share - 1)) >> depth) * nc + (to >> tall)) << depth) + (to & (d.rp - 1))
    order = onehot(iota((d.zb, d.zb), 0) == source)
    moved = dot(
        jnp.concatenate([normed[:, t * d.zb : (t + 1) * d.zb] for t in range(nz)], axis=0).astype(BF16),
        order).astype(BF16)
    for t in range(nz):
        for j in range(nc):
            qa_send[t * nc + j] = moved[t * PAD : (t + 1) * PAD, j * share : (j + 1) * share]
    lane = iota((8, d.nt), 1)
    field = iota((8, d.nt), 0)
    info = jnp.zeros((8, d.nt), F32)
    for r in range(b):
        here = lane == slot * line + z * b + r
        for j, number in enumerate((
            ids[0, r].astype(F32), ids[1, r].astype(F32), rw[0, r], rw[1, r],
        )):
            info = jnp.where(here & (field == j), number, info)
    info_a[...] = info
    pl.semaphore_wait(barrier, len(peers))

    pending = []

    def send(copy):
        copy.start()
        pending.append(copy)
        return copy

    def keep(number, src, dst):
        copy = pltpu.make_async_copy(src, dst, load_sem.at[number])
        copy.start()
        return copy

    zc = [(k, j) for k in far_first(nz) for j in range(nc)] + [(0, j) for j in range(1, nc)]
    me = z * nc + c

    def there(k, j):
        return up_z(k) * nc + up_c(j)

    def zc_exchange(base, source, everything):
        return [
            send(remote(
                source.at[there(k, j)], everything.at[me],
                zs.at[base + k * nc + j], zr.at[base + k * nc + j], z=up_z(k), c=up_c(j)))
            for k, j in zc
        ]

    own_rows = pl.multiple_of(y * d.rp, 8)
    own_piece = pl.multiple_of((y * nc + c) * d.rp, 8)

    def from_y(k):
        return lax.rem(y - k + ny, ny)

    wq_in = [
        send(remote(wq, wq_all.at[pl.ds(own_rows, d.rp)], ys.at[k], yr.at[k], y=up_y(k)))
        for k in far_first(ny)
    ]
    own_q = keep(5, wq, wq_all.at[pl.ds(own_rows, d.rp)])
    qa_in = zc_exchange(0, qa_send, qa_recv)
    own_a = keep(7, qa_send.at[me], qa_recv.at[me])
    info_in = [
        send(remote(info_a, info_az.at[z], zs.at[4 * nz + k], zr.at[4 * nz + k], z=up_z(k)))
        for k in far_first(nz)
    ]
    wo_in = {
        k: send(remote(wo, wo_all.at[pl.ds(own_piece, d.rp)], ys.at[ny + k], yr.at[ny + k], y=up_y(k)))
        for k in far_first(ny)
    }
    own_o = keep(6, wo, wo_all.at[pl.ds(own_piece, d.rp)])
    wo_fwd = [send(remote(wo, wo_all.at[pl.ds(own_piece, d.rp)], cs.at[0], cr.at[0], c=other))]
    ta_in = [
        send(remote(ta_send.at[up_z(k)], ta_recv.at[z], zs.at[5 * nz + k], zr.at[5 * nz + k], z=up_z(k)))
        for k in far_first(nz)
    ]
    own_t = keep(8, ta_send.at[z], ta_recv.at[z])

    for copy in qa_in:
        copy.wait_recv()
    own_a.wait()
    own_q.wait()
    rows_a = stacked(qa_recv, nz * nc)
    for copy in wq_in:
        copy.wait_recv()
    partial = dot(rows_a, wq_all[...]).astype(BF16)
    for t in range(nz * nc):
        qp_send[t] = partial[t * PAD : (t + 1) * PAD]
    qp_in = zc_exchange(2 * nz, qp_send, qp_recv)
    own_p = keep(9, qp_send.at[me], qp_recv.at[me])

    for k in near_first(ny):
        wo_in[k].wait_recv()
        part = wo_all.at[pl.ds(pl.multiple_of((from_y(k) * nc + c) * d.rp, 8), d.rp)]
        wo_fwd.append(send(remote(part, part, cs.at[k], cr.at[k], c=other)))
    for copy in info_in:
        copy.wait_recv()
    info = info_a[...]
    for k in range(1, nz):
        info = info + info_az[up_z(k)]
    info_b[...] = info
    info_y_in = [
        send(remote(info_b, info_by.at[y], ys.at[2 * ny + k], yr.at[2 * ny + k], y=up_y(k)))
        for k in far_first(ny)
    ]
    loads[0].wait()
    loads[1].wait()

    for copy in qp_in:
        copy.wait_recv()
    own_p.wait()
    q = qp_recv[0].astype(F32)
    for t in range(1, nz * nc):
        q = q + qp_recv[t].astype(F32)
    q = jnp.concatenate([q, jnp.zeros((8 - PAD, d.ql), F32)], axis=0)
    mixed = attention(d, q, kbuf, vbuf, lens, hoff)
    mx_send[...] = mixed[0:PAD]
    mx_in = [
        send(remote(mx_send, mx_recv.at[z], zs.at[6 * nz + k], zr.at[6 * nz + k], z=up_z(k)))
        for k in far_first(nz)
    ]
    own_m = keep(10, mx_send, mx_recv.at[z])

    for copy in info_y_in:
        copy.wait_recv()
    info = info_b[...]
    for k in range(1, ny):
        info = info + info_by[up_y(k)]
    info_c[...] = info
    info_c_in = send(remote(info_c, info_cc, cs.at[ny], cr.at[ny], c=other))

    pick_t = iota((line, nz * PAD), 0)
    pick_s = iota((line, nz * PAD), 1)
    within = pick_s & (PAD - 1)
    pick = onehot((within < b) & ((pick_s >> (PAD.bit_length() - 1)) * b + within == pick_t))
    for copy in ta_in:
        copy.wait_recv()
    own_t.wait()
    tok = dot(pick, stacked(ta_recv, nz))
    for copy in wo_fwd:
        copy.wait_recv()
    own_o.wait()
    for copy in mx_in:
        copy.wait_recv()
    own_m.wait()
    tight = dot(pick, stacked(mx_recv, nz)).astype(BF16)
    part = dot(tight, wo_all[...], ((1,), (1,)))
    pt_send[...] = part.astype(BF16)

    away = remote(pt_send, pt_recv.at[x], xs.at[0], xr.at[x], x=home)
    own_lanes = pl.multiple_of(lax.rem(z, d.nb) * d.zb, d.zb)
    own_block = line_rows.at[:, pl.ds(own_lanes, d.zb)]
    own_b = pltpu.make_async_copy(rb_send, own_block, load_sem.at[11])

    def to_line(k):
        return remote(
            rb_send, own_block, zs.at[7 * nz + k], zr.at[7 * nz + lax.rem(z, d.nb)], z=up_z(k))

    @pl.when(x != home)
    def _():
        away.start()

    @pl.when(x == home)
    def _():
        total = tok + pt_send[...].astype(F32)
        for k in range(1, nx):
            source = lax.rem(x + k, nx)
            remote(pt_send, pt_recv.at[source], xs.at[0], xr.at[source], x=source).wait_recv()
            total = total + pt_recv[source].astype(F32)
        rb_send[...] = total.astype(BF16)
        own_b.start()
        for k in far_first(nz):
            to_line(k).start()

    info_c_in.wait_recv()
    info = info_c[...] + info_cc[...]
    info_out[...] = info
    id0 = info[0:1]
    id1 = info[1:2]
    count = float(ny * nc)
    low = z.astype(F32) * count
    half_width = ny * line

    def line_of(places):
        return jnp.floor((places.astype(F32) + 0.5) * (1.0 / line))

    token_line = line_of(iota((1, d.nt), 1))
    token_half = jnp.where(token_line >= ny, 1.0, 0.0)
    ours = token_half == c.astype(F32)
    staying = (id0 >= low) & (id0 < low + count)
    stay = jnp.where(staying, 1.0, 0.0)
    hits = []
    for j in range(nc):
        expert = low + (y * nc + j).astype(F32)
        hits.append((jnp.where(id0 == expert, 1.0, 0.0), jnp.where(id1 == expert, 1.0, 0.0)))
    first, second = iota((d.nt, d.nt), 0), iota((d.nt, d.nt), 1)
    earlier = first < second
    same_line = line_of(first) == line_of(second)
    same_half = (first < half_width) == (second < half_width)
    line_rank = dot(jnp.broadcast_to(stay, (8, d.nt)).astype(BF16), onehot(earlier & same_line))[0:1]
    hit_rows = jnp.concatenate([h0 + h1 for h0, h1 in hits], axis=0)
    hit_rank = dot(hit_rows.astype(BF16), onehot(earlier & same_half))
    numbers = iota((SLOTS, d.nt), 0).astype(F32)
    chosen = [
        onehot((numbers == hit_rank[j : j + 1]) & (hit_rows[j : j + 1] > 0.5) & ours) for j in range(nc)
    ]
    routes = [h0 * info[2:3] + h1 * info[3:4] for h0, h1 in hits]
    slot_route = jnp.concatenate([
        jnp.sum(chosen[j].astype(F32) * routes[j], axis=1, keepdims=True) for j in range(nc)], axis=0)
    chosen = jnp.concatenate(chosen, axis=0)
    kept = ny * SLOTS
    place = (token_line - c.astype(F32) * ny) * SLOTS + line_rank
    packed = onehot(
        (iota((kept, d.nt), 0).astype(F32) == place) & staying & ours & (line_rank < SLOTS - 0.5))
    chosen = dot(chosen, packed, ((1,), (1,))).astype(BF16)
    own_token = onehot(iota((d.nt, line), 0) == iota((d.nt, line), 1) + slot * line)
    own_pack = dot(
        onehot((numbers == line_rank) & staying & (token_line == slot.astype(F32))), own_token).astype(BF16)
    spread_s = iota((nz * 8, line), 0)
    spread_t = iota((nz * 8, line), 1)
    spread = onehot(((spread_s & 7) < b) & ((spread_s >> 3) * b + (spread_s & 7) == spread_t))
    spread = dot(spread, own_pack, ((1,), (1,))).astype(BF16)
    expert = iota((d.experts, d.nt), 0).astype(F32)
    named = onehot((id0 == expert) | (id1 == expert))
    group_t = iota((d.nt, 128), 0)
    group_g = iota((d.nt, 128), 1)
    halves = dot(named, onehot((group_t >= half_width) == (group_g > 0)))
    zone = iota((8, d.nt), 0).astype(F32) * count
    lines = dot(onehot((id0 >= zone) & (id0 < zone + count)), onehot(line_of(group_t) == group_g.astype(F32)))
    most = jnp.maximum(jnp.max(halves), jnp.max(lines))
    most_out[0] = jnp.where(most > SLOTS, 1, 0)

    for j in range(d.nb):
        source = x * d.nb + j

        @pl.when(z != source)
        def _():
            block = line_rows.at[:, pl.ds(j * d.zb, d.zb)]
            remote(rb_send, block, zs.at[0], zr.at[7 * nz + j], z=source).wait_recv()

    @pl.when(x == home)
    def _():
        own_b.wait()

    save = keep(12, line_rows, line_out)
    own_send[...] = dot(own_pack, line_rows[...]).astype(BF16)
    own_slots = pl.ds(pl.multiple_of(y * SLOTS, SLOTS), SLOTS)
    rows_in = [
        send(remote(own_send, rows.at[own_slots], ys.at[3 * ny + k], yr.at[3 * ny + k], y=up_y(k)))
        for k in far_first(ny)
    ]
    own_s = keep(13, own_send, rows.at[own_slots])
    mine_t = iota((8, line), 1)
    mine_r = iota((8, line), 0)
    resid = dot(onehot((mine_r < b) & (mine_t == mine_r + z * b)), line_rows[...])
    own_s.wait()
    for copy in rows_in:
        copy.wait_recv()

    s_send[...] = dot(chosen, rows[...]).astype(BF16).reshape(nc, SLOTS, d.xs)
    xc = [(k, j) for k in far_first(nx) for j in range(nc)] + [(0, j) for j in range(1, nc)]
    our_slots = pl.ds(pl.multiple_of(c * SLOTS, SLOTS), SLOTS)
    s_in = [
        send(remote(
            s_send.at[up_c(j)], s_recv.at[x, our_slots],
            xs.at[1 + k * nc + j], xr.at[nx + k * nc + j], x=up_x(k), c=up_c(j)))
        for k, j in xc
    ]
    own_s = keep(5, s_send.at[c], s_recv.at[x, our_slots])
    for copy in loads[2:]:
        copy.wait()
    own_s.wait()
    for copy in s_in:
        copy.wait_recv()
    wide = [s_recv[t].astype(F32) for t in range(nx)]
    square = sum(jnp.sum(part * part, axis=1, keepdims=True) for part in wide)
    scale = lax.rsqrt(square / d.width + 1e-06)
    gated = jnp.zeros((nc * SLOTS, d.ff), F32)
    upward = jnp.zeros((nc * SLOTS, d.ff), F32)
    for t in range(nx):
        span = slice(t * d.xs, (t + 1) * d.xs)
        part = (wide[t] * scale * egain[:, span]).astype(BF16)
        gated = gated + dot(part, gbuf[span, :])
        upward = upward + dot(part, ubuf[span, :])
    hidden = (gated / (1.0 + jnp.exp(-gated)) * upward).astype(BF16)
    for t in range(nx):
        h_send[t] = dot(hidden, dbuf[:, t * d.xs : (t + 1) * d.xs]).astype(BF16)

    def to_half(j):
        return pl.ds(pl.multiple_of(up_c(j) * SLOTS, SLOTS), SLOTS)

    h_in = [
        send(remote(
            h_send.at[up_x(k), to_half(j)], h_recv.at[x, our_slots],
            xs.at[1 + nx * nc + k * nc + j], xr.at[nx + nx * nc + k * nc + j], x=up_x(k), c=up_c(j)))
        for k, j in xc
    ]
    own_h = keep(6, h_send.at[x, our_slots], h_recv.at[x, our_slots])
    own_h.wait()
    for copy in h_in:
        copy.wait_recv()
    total = h_recv[0].astype(F32)
    for t in range(1, nx):
        total = total + h_recv[t].astype(F32)
    answer = (total.astype(BF16).astype(F32) * slot_route).astype(BF16)
    y_send[...] = dot(chosen, answer, ((0,), (0,))).astype(BF16).reshape(ny, SLOTS, d.xs)
    y_in = [
        send(remote(y_send.at[up_y(k)], y_recv.at[y], ys.at[4 * ny + k], yr.at[4 * ny + k], y=up_y(k)))
        for k in far_first(ny)
    ]
    own_y = keep(7, y_send.at[y], y_recv.at[y])
    own_y.wait()
    for copy in y_in:
        copy.wait_recv()
    total = y_recv[0].astype(F32)
    for t in range(1, ny):
        total = total + y_recv[t].astype(F32)
    owned = dot(spread, total.astype(BF16)).astype(BF16)
    for t in range(nz):
        z_send[t] = owned[t * 8 : t * 8 + PAD]
    z_in = [
        send(remote(z_send.at[up_z(k)], z_recv.at[z], zs.at[8 * nz + k], zr.at[8 * nz + k], z=up_z(k)))
        for k in far_first(nz)
    ]
    own_z = keep(8, z_send.at[z], z_recv.at[z])
    save.wait()

    @pl.when(x != home)
    def _():
        away.wait_send()

    @pl.when(x == home)
    def _():
        for k in near_first(nz):
            to_line(k).wait_send()

    own_z.wait()
    for copy in z_in:
        copy.wait_recv()
    resid = resid[0:PAD]
    for t in range(nz):
        resid = resid + z_recv[t].astype(F32)
    out[...] = resid[0:b].astype(BF16)
    for copy in pending:
        copy.wait_send()


def layer(d, args):
    def vmem(*shape, dtype=BF16):
        return pltpu.VMEM(shape, dtype)

    line = d.nz * d.b
    dma = pltpu.SemaphoreType.DMA
    inside = pl.BlockSpec(memory_space=pltpu.VMEM)
    outside = pl.BlockSpec(memory_space=pltpu.HBM)
    return pl.pallas_call(
        functools.partial(kernel, d),
        out_shape=(
            jax.ShapeDtypeStruct((d.b, d.xs), BF16),
            jax.ShapeDtypeStruct((line, d.xs), BF16),
            jax.ShapeDtypeStruct((8, d.nt), F32),
            jax.ShapeDtypeStruct((1,), jnp.int32),
        ),
        in_specs=[outside] * 14,
        out_specs=(inside, outside, inside, pl.BlockSpec(memory_space=pltpu.SMEM)),
        scratch_shapes=[
            vmem(d.b, d.width), vmem(1, d.width, dtype=F32), vmem(d.rp, d.ql), vmem(d.rp, d.ql),
            vmem(1, d.width, dtype=F32),
            pltpu.SMEM((d.b,), jnp.int32), pltpu.SMEM((d.ql // d.hd,), F32),
            pltpu.SMEM((2, d.b), jnp.int32), pltpu.SMEM((2, d.b), F32),
            vmem(d.b, d.cache, d.hd), vmem(d.b, d.cache, d.hd),
            vmem(d.width, d.ff), vmem(d.width, d.ff), vmem(d.ff, d.width),
            dma((23,)),
            vmem(d.nz, PAD, d.zb), vmem(d.nz, PAD, d.zb),
            vmem(d.nz * d.nc, PAD, d.zb // d.nc), vmem(d.nz * d.nc, PAD, d.zb // d.nc),
            vmem(d.ny * d.rp, d.ql), vmem(d.zb, d.ql),
            vmem(d.nz * d.nc, PAD, d.ql), vmem(d.nz * d.nc, PAD, d.ql),
            vmem(PAD, d.ql), vmem(d.nz, PAD, d.ql),
            vmem(line, d.zb), vmem(d.nx, line, d.zb), vmem(line, d.zb),
            vmem(line, d.xs), vmem(SLOTS, d.xs), vmem(d.ny * SLOTS, d.xs),
            vmem(d.nc, SLOTS, d.xs), vmem(d.nx, d.nc * SLOTS, d.xs),
            vmem(d.nx, d.nc * SLOTS, d.xs), vmem(d.nx, d.nc * SLOTS, d.xs),
            vmem(d.ny, SLOTS, d.xs), vmem(d.ny, SLOTS, d.xs),
            vmem(d.nz, PAD, d.xs), vmem(d.nz, PAD, d.xs),
            vmem(8, d.nt, dtype=F32), vmem(d.nz, 8, d.nt, dtype=F32),
            vmem(8, d.nt, dtype=F32), vmem(d.ny, 8, d.nt, dtype=F32),
            vmem(8, d.nt, dtype=F32), vmem(8, d.nt, dtype=F32),
            dma((9 * d.nz,)), dma((9 * d.nz,)),
            dma((5 * d.ny,)), dma((5 * d.ny,)),
            dma((1 + 2 * d.nx * d.nc,)), dma((d.nx + 2 * d.nx * d.nc,)),
            dma((d.ny + 1,)), dma((d.ny + 1,)),
        ],
        compiler_params=pltpu.CompilerParams(
            collective_id=0, has_side_effects=True, vmem_limit_bytes=60 * 1024 * 1024),
    )(*args)


def crowded(d, line, info, expert_gain, gate_weight, up_weight, down_weight):
    places = ("c", "y")
    copies = jnp.broadcast_to(line, (d.nc * d.ny, *line.shape))
    lines = lax.all_to_all(copies, places, split_axis=0, concat_axis=0, tiled=True)
    rows = lines.reshape(d.nt, d.xs)
    copies = jnp.broadcast_to(rows, (d.nx, *rows.shape))
    spans = lax.all_to_all(copies, "x", split_axis=0, concat_axis=0, tiled=True)
    full = jnp.moveaxis(spans, 0, 1).reshape(d.nt, d.width)
    wide = full.astype(F32)
    scale = lax.rsqrt(jnp.mean(wide * wide, axis=-1, keepdims=True) + 1e-06)
    normed = (wide * scale * expert_gain).astype(BF16)
    gated = jnp.dot(normed, gate_weight, preferred_element_type=F32)
    upward = jnp.dot(normed, up_weight, preferred_element_type=F32)
    hidden = (jax.nn.silu(gated) * upward).astype(BF16)
    term = jnp.dot(hidden, down_weight, preferred_element_type=F32).astype(BF16)
    tiles = jnp.moveaxis(term.reshape(d.nt, d.nx, d.xs), 1, 0)
    terms = lax.all_to_all(tiles, "x", split_axis=0, concat_axis=0, tiled=True)
    answer = terms.astype(F32).sum(axis=0).astype(BF16).astype(F32)
    mine = lax.axis_index(EP).astype(F32)
    route = jnp.where(info[0] == mine, info[2], 0.0) + jnp.where(info[1] == mine, info[3], 0.0)
    answer = answer * route[:, None]
    answer = answer.reshape(d.nc, d.ny, d.nz, d.b, d.xs).transpose(2, 1, 0, 3, 4)
    answer = answer.reshape(-1, d.b, d.xs)
    back = lax.all_to_all(answer, EP, split_axis=0, concat_axis=0, tiled=True)
    z, y, c = (lax.axis_index(name) for name in EP)
    first = ((c * d.ny + y) * d.nz + z) * d.b
    resid = lax.dynamic_slice_in_dim(rows, first, d.b, 0)
    return (resid.astype(F32) + back.sum(axis=0)).astype(BF16)


def local(
    tokens,
    mixer_gain,
    query_weight,
    key_cache,
    value_cache,
    seq_lengths,
    head_offset,
    output_weight,
    expert_gain,
    expert_ids,
    route_weight,
    gate_weight,
    up_weight,
    down_weight,
):
    nz, ny, nc, nx = (lax.axis_size(name) for name in ("z", "y", "c", "x"))
    batch, width = tokens.shape
    d = SimpleNamespace(
        nz=nz, ny=ny, nc=nc, nx=nx, b=batch, width=width, zb=width // nz, xs=width // nx,
        nb=nz // nx, rp=query_weight.shape[0], ql=query_weight.shape[1], hd=key_cache.shape[3],
        cache=key_cache.shape[1], ff=gate_weight.shape[2], nt=nz * ny * nc * batch,
        experts=nz * ny * nc,
    )
    done, line, info, most = layer(d, (
        tokens,
        mixer_gain.reshape(1, width),
        query_weight,
        key_cache.reshape(batch, d.cache, d.hd),
        value_cache.reshape(batch, d.cache, d.hd),
        seq_lengths,
        head_offset,
        output_weight.T,
        expert_gain.reshape(1, width),
        expert_ids.T,
        route_weight.T,
        gate_weight[0],
        up_weight[0],
        down_weight[0],
    ))
    return lax.cond(
        most[0] > 0,
        lambda: crowded(d, line, info, expert_gain, gate_weight[0], up_weight[0], down_weight[0]),
        lambda: done,
    )


def solution(mesh):
    split = Mesh(mesh.devices.reshape(8, 8, 2, mesh.shape["tp"]), ("z", "y", "c", "x"))
    return sharded(split)


def sharded(split):
    in_specs = (
        P(EP, None),
        P(),
        P(EP, "x"),
        P(EP, None, "x", None),
        P(EP, None, "x", None),
        P(EP),
        P("x"),
        P("x", EP),
        P(),
        P(EP, None),
        P(EP, None),
        P(EP, None, "x"),
        P(EP, None, "x"),
        P(EP, "x", None),
    )
    return jax.shard_map(local, mesh=split, in_specs=in_specs, out_specs=P(EP, "x"), check_vma=False)
```

profile of v0, /device:TPU:1, one launch (start us, length us, event | category | flops | bytes accessed | tf_op | source)
XLA Modules:
  0.0 68.4 jit_solution(12621103425664367075)
XLA Ops:
  0.0 0.0 copy-start.1
  0.0 66.5 %shard_map.138 = (bf16[3,512]{1,0:T(4,128)(2,1)}, bf16[24,512]{1,0:T(8,128)(2,1)S(1)}, f32[8,384]{1,0:T(8,128)}, s32[1]{0:T(128)}) custom-call(bf16[3,2048]{1,0:T(4,128)(2,1)} %refs_0_.1, f32[1,2048]{1,0:T(1,128)} %bitcast.49, bf16[16,512]{1,0:T(8,128)(2,1)} %refs_2_.1, bf16[3,1024,128]{2,1,0:T(8,128)(2,1)} %bitcast.45, bf16[3,1024,128]{2,1,0:T(8,128)(2,1)} %bitcast.46, ...), custom_call_target="tpu_custom_call" | custom-call | tf_op jit(solution)/shard_map/pallas_call | solution.py:514
  67.1 0.0 copy-done.1
  67.1 1.3 %copy.35 = bf16[3,512]{1,0:T(4,128)(2,1)} copy(bf16[3,512]{1,0:T(4,128)(2,1)} %get-tuple-element.35) | data formatting | bytes 6144
  (1 shorter events, 0.0 us)
Async XLA Ops:
  0.0 67.1 %copy-start.1 = (f32[2048]{0:T(1024)S(1)}, f32[2048]{0:T(1024)}, u32[]{:S(2)}) copy-start(f32[2048]{0:T(1024)} %param.24) | copy-start | bytes 24580
where the time goes:
time: 68.7 us; the launch traced here: 68.4 us
  Pallas kernels  66.5 us (97%)
  local copies, waits for them, and re-layouts  1.27 us (2%)
    pallas_call x1, Pallas kernels, layer(): pl.pallas_call(functools.partial(kernel, d), out_shape=(jax.ShapeDtypeStr...  66.5 us

commit v1 on v0

--- a/solution.py
+++ b/solution.py
@@ -38,6 +38,21 @@
 
 def stacked(ref, count):
     return jnp.concatenate([ref[t].astype(F32) for t in range(count)], axis=0).astype(BF16)
+
+
+def turned(value):
+    return jnp.concatenate([value[:, 64:], value[:, :64]], axis=1)
+
+
+def side_by_side(d, upper, lower):
+    low = iota((upper.shape[0], 128), 1) < 64
+    result = []
+    for t in range(d.nx):
+        span = slice(t // 2 * 128, t // 2 * 128 + 128)
+        left, right = upper[:, span], lower[:, span]
+        pair = (left, turned(right)) if t % 2 == 0 else (turned(left), right)
+        result.append(jnp.where(low, *pair).astype(BF16))
+    return result
 
 
 def remote(src, dst, send_sem, recv_sem, **where):
@@ -96,10 +111,11 @@
     (tokens, mgain, wq, wo, egain, lens, hoff, ids, rw,
      kbuf, vbuf, gbuf, ubuf, dbuf, load_sem,
      ta_send, ta_recv, qa_send, qa_recv, wq_all, wo_all, qp_send, qp_recv, mx_send, mx_recv,
+     tk_all, tk_recv, f_send, f_recv, gains,
      pt_send, pt_recv, rb_send, line_rows, own_send, rows, s_send, s_recv, h_send, h_recv,
-     y_send, y_recv, z_send, z_recv,
+     y_send, y_recv,
      info_a, info_az, info_b, info_by, info_c, info_cc,
-     zs, zr, ys, yr, xs, xr, cs, cr) = refs[18:]
+     zs, zr, ys, yr, xs, xr, cs, cr, fs, fr, gs, gr) = refs[18:]
     z, y, c, x = (lax.axis_index(name) for name in ("z", "y", "c", "x"))
     nz, ny, nc, nx, b = d.nz, d.ny, d.nc, d.nx, d.b
     other = 1 - c
@@ -120,15 +136,6 @@
     def up_c(k):
         return lax.rem(c + k, nc)
 
-    small = [
-        pltpu.make_async_copy(src, dst, load_sem.at[14 + i])
-        for i, (src, dst) in enumerate([
-            (tokens_in, tokens), (mgain_in, mgain), (wq_in_hbm, wq), (ids_in, ids), (rw_in, rw),
-            (wo_in_hbm, wo), (lens_in, lens), (hoff_in, hoff), (egain_in, egain),
-        ])
-    ]
-    for copy in small:
-        copy.start()
     barrier = pltpu.get_barrier_semaphore()
     peers = [{"z": up_z(k), "c": up_c(j)} for k in far_first(nz) for j in range(nc)]
     peers += [{"y": up_y(k)} for k in far_first(ny)]
@@ -137,15 +144,45 @@
     for peer in peers:
         pl.semaphore_signal(barrier, inc=1, device_id=peer, device_id_type=MESH)
 
+    small = [
+        pltpu.make_async_copy(src, dst, load_sem.at[14 + i])
+        for i, (src, dst) in enumerate([
+            (tokens_in, tokens), (mgain_in, mgain), (wq_in_hbm, wq), (ids_in, ids), (rw_in, rw),
+            (wo_in_hbm, wo), (lens_in, lens), (hoff_in, hoff), (egain_in, egain),
+        ])
+    ]
+    for copy in small:
+        copy.start()
+    loads = [(key, kbuf), (val, vbuf), (down, dbuf)]
+    for t in range(nx):
+        loads += [(gate.at[:, t], gbuf.at[t]), (up.at[:, t], ubuf.at[t])]
     loads = [
-        pltpu.make_async_copy(src, dst, load_sem.at[i])
-        for i, (src, dst) in enumerate(
-            [(key, kbuf), (val, vbuf), (gate, gbuf), (up, ubuf), (down, dbuf)]
-        )
+        pltpu.make_async_copy(src, dst, load_sem.at[23 + i]) for i, (src, dst) in enumerate(loads)
     ]
     for copy in loads:
         copy.start()
-    for copy in small:
+    small[2].wait()
+    pl.semaphore_wait(barrier, len(peers))
+    pending = []
+
+    def send(copy):
+        copy.start()
+        pending.append(copy)
+        return copy
+
+    def keep(number, src, dst):
+        copy = pltpu.make_async_copy(src, dst, load_sem.at[number])
+        copy.start()
+        return copy
+
+    own_rows = pl.multiple_of(y * d.rp, 8)
+    own_piece = pl.multiple_of((y * nc + c) * d.rp, 8)
+    wq_in = [
+        send(remote(wq, wq_all.at[pl.ds(own_rows, d.rp)], ys.at[k], yr.at[k], y=up_y(k)))
+        for k in far_first(ny)
+    ]
+    own_q = keep(5, wq, wq_all.at[pl.ds(own_rows, d.rp)])
+    for copy in small[:2] + small[3:]:
         copy.wait()
 
     wide = tokens[...].astype(F32)
@@ -177,20 +214,6 @@
         )):
             info = jnp.where(here & (field == j), number, info)
     info_a[...] = info
-    pl.semaphore_wait(barrier, len(peers))
-
-    pending = []
-
-    def send(copy):
-        copy.start()
-        pending.append(copy)
-        return copy
-
-    def keep(number, src, dst):
-        copy = pltpu.make_async_copy(src, dst, load_sem.at[number])
-        copy.start()
-        return copy
-
     zc = [(k, j) for k in far_first(nz) for j in range(nc)] + [(0, j) for j in range(1, nc)]
     me = z * nc + c
 
@@ -205,17 +228,9 @@
             for k, j in zc
         ]
 
-    own_rows = pl.multiple_of(y * d.rp, 8)
-    own_piece = pl.multiple_of((y * nc + c) * d.rp, 8)
-
     def from_y(k):
         return lax.rem(y - k + ny, ny)
 
-    wq_in = [
-        send(remote(wq, wq_all.at[pl.ds(own_rows, d.rp)], ys.at[k], yr.at[k], y=up_y(k)))
-        for k in far_first(ny)
-    ]
-    own_q = keep(5, wq, wq_all.at[pl.ds(own_rows, d.rp)])
     qa_in = zc_exchange(0, qa_send, qa_recv)
     own_a = keep(7, qa_send.at[me], qa_recv.at[me])
     info_in = [
@@ -295,15 +310,50 @@
         copy.wait_recv()
     own_t.wait()
     tok = dot(pick, stacked(ta_recv, nz))
+    own_token = onehot(iota((d.nt, line), 0) == iota((d.nt, line), 1) + slot * line)
+    count = float(ny * nc)
+    own_ids = dot(info_b[...].astype(BF16), own_token)[0:1]
+    zone = iota((8, line), 0).astype(F32) * count
+    bound = onehot((own_ids >= zone) & (own_ids < zone + count))
+    bound_rank = dot(bound, onehot(iota((line, line), 0) < iota((line, line), 1)))
+    wide_rows = nz * SLOTS // 2
+    widen = onehot((iota((wide_rows, 8), 0) >> 3) == iota((wide_rows, 8), 1))
+    bound = dot(widen, bound) > 0.5
+    bound_rank = dot(widen, bound_rank.astype(BF16))
+    number = (iota((wide_rows, line), 0) & 7).astype(F32)
+    pack_all = jnp.concatenate(
+        [onehot(bound & (bound_rank == number)), onehot(bound & (bound_rank == number + 8.0))], axis=0)
+    moved = dot(pack_all, tok.astype(BF16))
+    for t, part in enumerate(side_by_side(d, moved[:wide_rows], moved[wide_rows:])):
+        tk_all[t] = part.reshape(nz, SLOTS // 2, 128)
+    tk_in = [
+        send(remote(tk_all.at[x, up_z(k)], tk_recv.at[z], zs.at[9 * nz + k], zr.at[9 * nz + k], z=up_z(k)))
+        for k in far_first(nz)
+    ]
+    own_tk = keep(0, tk_all.at[x, z], tk_recv.at[z])
+    pack_all = dot(pack_all, pick).astype(BF16)
+    for t in range(nx):
+        gains[t] = jnp.concatenate(
+            [egain[:, u * d.zb + t * 64 : u * d.zb + t * 64 + 64] for u in range(nz)], axis=1)
     for copy in wo_fwd:
         copy.wait_recv()
     own_o.wait()
     for copy in mx_in:
         copy.wait_recv()
     own_m.wait()
-    tight = dot(pick, stacked(mx_recv, nz)).astype(BF16)
-    part = dot(tight, wo_all[...], ((1,), (1,)))
-    pt_send[...] = part.astype(BF16)
+    all_mixed = stacked(mx_recv, nz)
+    moved = dot(dot(pack_all, all_mixed).astype(BF16), wo_all[...], ((1,), (1,)))
+    for t, part in enumerate(side_by_side(d, moved[:wide_rows], moved[wide_rows:])):
+        f_send[t] = part.reshape(nz, SLOTS // 2, 128)
+    f_in = [
+        send(remote(
+            f_send.at[up_x(j), up_z(k)], f_recv.at[x, z],
+            fs.at[k * nx + j], fr.at[k * nx + j], x=up_x(j), z=up_z(k)))
+        for k in far_first(nz) + [0] for j in far_first(nx) + [0] if k or j
+    ]
+    own_f = keep(1, f_send.at[x, z], f_recv.at[x, z])
+    tight = dot(pick, all_mixed).astype(BF16)
+    pt_send[...] = dot(tight, wo_all[...], ((1,), (1,))).astype(BF16)
 
     away = remote(pt_send, pt_recv.at[x], xs.at[0], xr.at[x], x=home)
     own_lanes = pl.multiple_of(lax.rem(z, d.nb) * d.zb, d.zb)
@@ -317,25 +367,12 @@
     @pl.when(x != home)
     def _():
         away.start()
-
-    @pl.when(x == home)
-    def _():
-        total = tok + pt_send[...].astype(F32)
-        for k in range(1, nx):
-            source = lax.rem(x + k, nx)
-            remote(pt_send, pt_recv.at[source], xs.at[0], xr.at[source], x=source).wait_recv()
-            total = total + pt_recv[source].astype(F32)
-        rb_send[...] = total.astype(BF16)
-        own_b.start()
-        for k in far_first(nz):
-            to_line(k).start()
 
     info_c_in.wait_recv()
     info = info_c[...] + info_cc[...]
     info_out[...] = info
     id0 = info[0:1]
     id1 = info[1:2]
-    count = float(ny * nc)
     low = z.astype(F32) * count
     half_width = ny * line
 
@@ -370,14 +407,19 @@
     place = (token_line - c.astype(F32) * ny) * SLOTS + line_rank
     packed = onehot(
         (iota((kept, d.nt), 0).astype(F32) == place) & staying & ours & (line_rank < SLOTS - 0.5))
+    chosen_tokens = chosen
     chosen = dot(chosen, packed, ((1,), (1,))).astype(BF16)
-    own_token = onehot(iota((d.nt, line), 0) == iota((d.nt, line), 1) + slot * line)
-    own_pack = dot(
-        onehot((numbers == line_rank) & staying & (token_line == slot.astype(F32))), own_token).astype(BF16)
-    spread_s = iota((nz * 8, line), 0)
-    spread_t = iota((nz * 8, line), 1)
-    spread = onehot(((spread_s & 7) < b) & ((spread_s >> 3) * b + (spread_s & 7) == spread_t))
-    spread = dot(spread, own_pack, ((1,), (1,))).astype(BF16)
+    owner_s = iota((ny * nz * PAD, d.nt), 0)
+    owner_t = iota((ny * nz * PAD, d.nt), 1) - c * half_width
+    r_of = owner_s & (PAD - 1)
+    first_of = (owner_s >> (PAD.bit_length() - 1)) * b
+    owners = onehot((r_of < b) & (first_of + r_of == owner_t))
+    owners = dot(owners, chosen_tokens, ((1,), (1,)))
+    homes = []
+    for r in range(b):
+        last = onehot((r_of == b) & (first_of + r == owner_t))
+        last = dot(last, chosen_tokens, ((1,), (1,)))
+        homes.append(jnp.concatenate([owners, last], axis=1).astype(BF16))
     expert = iota((d.experts, d.nt), 0).astype(F32)
     named = onehot((id0 == expert) | (id1 == expert))
     group_t = iota((d.nt, 128), 0)
@@ -388,29 +430,42 @@
     most = jnp.maximum(jnp.max(halves), jnp.max(lines))
     most_out[0] = jnp.where(most > SLOTS, 1, 0)
 
-    for j in range(d.nb):
-        source = x * d.nb + j
-
-        @pl.when(z != source)
-        def _():
-            block = line_rows.at[:, pl.ds(j * d.zb, d.zb)]
-            remote(rb_send, block, zs.at[0], zr.at[7 * nz + j], z=source).wait_recv()
-
-    @pl.when(x == home)
-    def _():
-        own_b.wait()
-
-    save = keep(12, line_rows, line_out)
-    own_send[...] = dot(own_pack, line_rows[...]).astype(BF16)
+    own_tk.wait()
+    for copy in tk_in:
+        copy.wait_recv()
+    own_f.wait()
+    for copy in f_in:
+        copy.wait_recv()
+    summed = []
+    for u in range(nz):
+        total = tk_recv[u].astype(F32)
+        for t in range(nx):
+            total = total + f_recv[t, u].astype(F32)
+        summed.append(total)
+    low_lanes = iota((SLOTS // 2, 128), 1) < 64
+    for u in range(0, nz, 2):
+        span = slice(u * 64, u * 64 + 128)
+        own_send[:, span] = jnp.concatenate([
+            jnp.where(low_lanes, summed[u], turned(summed[u + 1])),
+            jnp.where(low_lanes, turned(summed[u]), summed[u + 1])], axis=0).astype(BF16)
     own_slots = pl.ds(pl.multiple_of(y * SLOTS, SLOTS), SLOTS)
     rows_in = [
         send(remote(own_send, rows.at[own_slots], ys.at[3 * ny + k], yr.at[3 * ny + k], y=up_y(k)))
         for k in far_first(ny)
     ]
     own_s = keep(13, own_send, rows.at[own_slots])
-    mine_t = iota((8, line), 1)
-    mine_r = iota((8, line), 0)
-    resid = dot(onehot((mine_r < b) & (mine_t == mine_r + z * b)), line_rows[...])
+    @pl.when(x == home)
+    def _():
+        total = tok + pt_send[...].astype(F32)
+        for k in range(1, nx):
+            source = lax.rem(x + k, nx)
+            remote(pt_send, pt_recv.at[source], xs.at[0], xr.at[source], x=source).wait_recv()
+            total = total + pt_recv[source].astype(F32)
+        rb_send[...] = total.astype(BF16)
+        own_b.start()
+        for k in far_first(nz):
+            to_line(k).start()
+
     own_s.wait()
     for copy in rows_in:
         copy.wait_recv()
@@ -436,10 +491,9 @@
     gated = jnp.zeros((nc * SLOTS, d.ff), F32)
     upward = jnp.zeros((nc * SLOTS, d.ff), F32)
     for t in range(nx):
-        span = slice(t * d.xs, (t + 1) * d.xs)
-        part = (wide[t] * scale * egain[:, span]).astype(BF16)
-        gated = gated + dot(part, gbuf[span, :])
-        upward = upward + dot(part, ubuf[span, :])
+        part = (wide[t] * scale * gains[t]).astype(BF16)
+        gated = gated + dot(part, gbuf[t].reshape(d.xs, d.ff))
+        upward = upward + dot(part, ubuf[t].reshape(d.xs, d.ff))
     hidden = (gated / (1.0 + jnp.exp(-gated)) * upward).astype(BF16)
     for t in range(nx):
         h_send[t] = dot(hidden, dbuf[:, t * d.xs : (t + 1) * d.xs]).astype(BF16)
@@ -460,27 +514,44 @@
     total = h_recv[0].astype(F32)
     for t in range(1, nx):
         total = total + h_recv[t].astype(F32)
-    answer = (total.astype(BF16).astype(F32) * slot_route).astype(BF16)
-    y_send[...] = dot(chosen, answer, ((0,), (0,))).astype(BF16).reshape(ny, SLOTS, d.xs)
-    y_in = [
-        send(remote(y_send.at[up_y(k)], y_recv.at[y], ys.at[4 * ny + k], yr.at[4 * ny + k], y=up_y(k)))
-        for k in far_first(ny)
-    ]
-    own_y = keep(7, y_send.at[y], y_recv.at[y])
-    own_y.wait()
-    for copy in y_in:
-        copy.wait_recv()
-    total = y_recv[0].astype(F32)
-    for t in range(1, ny):
-        total = total + y_recv[t].astype(F32)
-    owned = dot(spread, total.astype(BF16)).astype(BF16)
+    answer = total.astype(BF16).astype(F32) * slot_route
+    part = d.xs // PAD
+    for r in range(b):
+        both = jnp.concatenate([answer[:, r * part : (r + 1) * part], answer[:, b * part :]], axis=0)
+        y_send[:, :, r * part : (r + 1) * part] = (
+            dot(homes[r], both.astype(BF16)).reshape(ny * nz, PAD, part).astype(BF16))
+
+    def give(t, k):
+        return remote(
+            y_send.at[up_y(k) * nz + t], y_recv.at[y * nz + z],
+            gs.at[t * ny + k], gr.at[z * ny + k], z=t, y=up_y(k))
+
     for t in range(nz):
-        z_send[t] = owned[t * 8 : t * 8 + PAD]
-    z_in = [
-        send(remote(z_send.at[up_z(k)], z_recv.at[z], zs.at[8 * nz + k], zr.at[8 * nz + k], z=up_z(k)))
-        for k in far_first(nz)
-    ]
-    own_z = keep(8, z_send.at[z], z_recv.at[z])
+        for k in far_first(ny):
+            send(give(t, k))
+
+        @pl.when(z != t)
+        def _():
+            give(t, 0).start()
+
+    given = nz * (ny - 1)
+    own_y = keep(7, y_send.at[y * nz + z], y_recv.at[y * nz + z])
+    for j in range(d.nb):
+        source = x * d.nb + j
+
+        @pl.when(z != source)
+        def _():
+            block = line_rows.at[:, pl.ds(j * d.zb, d.zb)]
+            remote(rb_send, block, zs.at[0], zr.at[7 * nz + j], z=source).wait_recv()
+
+    @pl.when(x == home)
+    def _():
+        own_b.wait()
+
+    save = keep(12, line_rows, line_out)
+    mine_t = iota((8, line), 1)
+    mine_r = iota((8, line), 0)
+    resid = dot(onehot((mine_r < b) & (mine_t == mine_r + z * b)), line_rows[...])
     save.wait()
 
     @pl.when(x != home)
@@ -492,14 +563,31 @@
         for k in near_first(nz):
             to_line(k).wait_send()
 
-    own_z.wait()
-    for copy in z_in:
-        copy.wait_recv()
-    resid = resid[0:PAD]
+    for copy in pending[:-given]:
+        copy.wait_send()
+    own_y.wait()
     for t in range(nz):
-        resid = resid + z_recv[t].astype(F32)
-    out[...] = resid[0:b].astype(BF16)
-    for copy in pending:
+        for k in near_first(ny):
+            remote(
+                y_send.at[0], y_recv.at[from_y(k) * nz + t], gs.at[0], gr.at[t * ny + k],
+                z=t, y=from_y(k)).wait_recv()
+
+        @pl.when(z != t)
+        def _():
+            remote(
+                y_send.at[0], y_recv.at[y * nz + t], gs.at[0], gr.at[t * ny], z=t).wait_recv()
+
+    total = y_recv[0].astype(F32)
+    for t in range(1, ny * nz):
+        total = total + y_recv[t].astype(F32)
+    last = jnp.concatenate([total[b : b + 1, r * part : (r + 1) * part] for r in range(b)], axis=0)
+    out[...] = (resid[0:b] + jnp.concatenate([total[0:b], last], axis=1)).astype(BF16)
+    for t in range(nz):
+        @pl.when(z != t)
+        def _():
+            give(t, 0).wait_send()
+
+    for copy in pending[-given:]:
         copy.wait_send()
 
 
@@ -514,7 +602,7 @@
     return pl.pallas_call(
         functools.partial(kernel, d),
         out_shape=(
-            jax.ShapeDtypeStruct((d.b, d.xs), BF16),
+            pltpu.VMEM((d.b, d.xs), BF16),
             jax.ShapeDtypeStruct((line, d.xs), BF16),
             jax.ShapeDtypeStruct((8, d.nt), F32),
             jax.ShapeDtypeStruct((1,), jnp.int32),
@@ -527,26 +615,30 @@
             pltpu.SMEM((d.b,), jnp.int32), pltpu.SMEM((d.ql // d.hd,), F32),
             pltpu.SMEM((2, d.b), jnp.int32), pltpu.SMEM((2, d.b), F32),
             vmem(d.b, d.cache, d.hd), vmem(d.b, d.cache, d.hd),
-            vmem(d.width, d.ff), vmem(d.width, d.ff), vmem(d.ff, d.width),
-            dma((23,)),
+            vmem(d.nx, d.nz, d.zb // d.nx, d.ff), vmem(d.nx, d.nz, d.zb // d.nx, d.ff), vmem(d.ff, d.width),
+            dma((26 + 2 * d.nx,)),
             vmem(d.nz, PAD, d.zb), vmem(d.nz, PAD, d.zb),
             vmem(d.nz * d.nc, PAD, d.zb // d.nc), vmem(d.nz * d.nc, PAD, d.zb // d.nc),
             vmem(d.ny * d.rp, d.ql), vmem(d.zb, d.ql),
             vmem(d.nz * d.nc, PAD, d.ql), vmem(d.nz * d.nc, PAD, d.ql),
             vmem(PAD, d.ql), vmem(d.nz, PAD, d.ql),
+            vmem(d.nx, d.nz, SLOTS // 2, 128), vmem(d.nz, SLOTS // 2, 128),
+            vmem(d.nx, d.nz, SLOTS // 2, 128), vmem(d.nx, d.nz, SLOTS // 2, 128),
+            vmem(d.nx, 1, d.xs, dtype=F32),
             vmem(line, d.zb), vmem(d.nx, line, d.zb), vmem(line, d.zb),
             vmem(line, d.xs), vmem(SLOTS, d.xs), vmem(d.ny * SLOTS, d.xs),
             vmem(d.nc, SLOTS, d.xs), vmem(d.nx, d.nc * SLOTS, d.xs),
             vmem(d.nx, d.nc * SLOTS, d.xs), vmem(d.nx, d.nc * SLOTS, d.xs),
-            vmem(d.ny, SLOTS, d.xs), vmem(d.ny, SLOTS, d.xs),
-            vmem(d.nz, PAD, d.xs), vmem(d.nz, PAD, d.xs),
+            vmem(d.ny * d.nz, PAD, d.xs // PAD * d.b), vmem(d.ny * d.nz, PAD, d.xs // PAD * d.b),
             vmem(8, d.nt, dtype=F32), vmem(d.nz, 8, d.nt, dtype=F32),
             vmem(8, d.nt, dtype=F32), vmem(d.ny, 8, d.nt, dtype=F32),
             vmem(8, d.nt, dtype=F32), vmem(8, d.nt, dtype=F32),
-            dma((9 * d.nz,)), dma((9 * d.nz,)),
+            dma((10 * d.nz,)), dma((10 * d.nz,)),
             dma((5 * d.ny,)), dma((5 * d.ny,)),
             dma((1 + 2 * d.nx * d.nc,)), dma((d.nx + 2 * d.nx * d.nc,)),
             dma((d.ny + 1,)), dma((d.ny + 1,)),
+            dma((d.nz * d.nx,)), dma((d.nz * d.nx,)),
+            dma((d.nz * d.ny,)), dma((d.nz * d.ny,)),
         ],
         compiler_params=pltpu.CompilerParams(
             collective_id=0, has_side_effects=True, vmem_limit_bytes=60 * 1024 * 1024),
@@ -619,8 +711,8 @@
         expert_gain.reshape(1, width),
         expert_ids.T,
         route_weight.T,
-        gate_weight[0],
-        up_weight[0],
+        gate_weight.reshape(nz, nx, d.zb // nx, d.ff),
+        up_weight.reshape(nz, nx, d.zb // nx, d.ff),
         down_weight[0],
     ))
     return lax.cond(

time: 68.7 us -> 65.7 us (0.956)
  Pallas kernels: 66.5 us -> 64.3 us
    pallas_call x1, Pallas kernels: 66.5 us -> 64.3 us  [layer(): pl.pallas_call(functools.partial(kernel, d), out_shape=(pltpu.VMEM((d.b,...]
where the time goes in v1:
time: 65.7 us; the launch traced here: 65.6 us
  Pallas kernels  64.3 us (98%)
  between operations  0.66 us (1%)
    pallas_call x1, Pallas kernels, layer(): pl.pallas_call(functools.partial(kernel, d), out_shape=(pltpu.VMEM((d.b,...  64.3 us

profile of v1, /device:TPU:1, one launch (start us, length us, event | category | flops | bytes accessed | tf_op | source)
XLA Modules:
  0.0 65.6 jit_solution(15525016349211198235)
XLA Ops:
  0.0 0.0 copy-start.1
  0.0 64.3 %shard_map.138 = (bf16[3,512]{1,0:T(4,128)(2,1)S(1)}, bf16[24,512]{1,0:T(8,128)(2,1)S(1)}, f32[8,384]{1,0:T(8,128)}, s32[1]{0:T(128)}) custom-call(bf16[3,2048]{1,0:T(4,128)(2,1)} %refs_0_.1, f32[1,2048]{1,0:T(1,128)} %bitcast.49, bf16[16,512]{1,0:T(8,128)(2,1)} %refs_2_.1, bf16[3,1024,128]{2,1,0:T(8,128)(2,1)} %bitcast.45, bf16[3,1024,128]{2,1,0:T(8,128)(2,1)} %bitcast.46, ...), custom_call_target="tpu_custom_call" | custom-call | tf_op jit(solution)/shard_map/pallas_call | solution.py:602
  64.9 0.0 copy-done.1
  65.0 0.6 copy.35
  (1 shorter events, 0.0 us)
Async XLA Ops:
  0.0 64.9 %copy-start.1 = (f32[2048]{0:T(1024)S(1)}, f32[2048]{0:T(1024)}, u32[]{:S(2)}) copy-start(f32[2048]{0:T(1024)} %param.24) | copy-start | bytes 24580

commit v2 on v1

--- a/solution.py
+++ b/solution.py
@@ -68,12 +68,12 @@
 
 def attention(d, q, kbuf, vbuf, lens, hoff):
     heads = d.ql // d.hd
-    rows = heads * 8
+    rows = heads * PAD
     queries = jnp.concatenate([q[:, h * d.hd : (h + 1) * d.hd] for h in range(heads)], axis=0)
     queries = queries.astype(BF16)
     row = iota((rows, 1), 0)
-    seq = row & 7
-    head = row >> 3
+    seq = row & (PAD - 1)
+    head = row >> (PAD.bit_length() - 1)
     score = jnp.zeros((rows, d.cache), F32)
     length = jnp.zeros((rows, 1), jnp.int32)
     offset = jnp.zeros((rows, 1), F32)
@@ -101,7 +101,7 @@
     total = jnp.zeros((rows, d.hd), F32)
     for b in range(d.b):
         total = jnp.where(seq == b, dot(weight, vbuf[b]), total)
-    return jnp.concatenate([total[h * 8 : (h + 1) * 8] for h in range(heads)], axis=1).astype(BF16)
+    return jnp.concatenate([total[h * PAD : (h + 1) * PAD] for h in range(heads)], axis=1).astype(BF16)
 
 
 def kernel(d, *refs):
@@ -114,7 +114,7 @@
      tk_all, tk_recv, f_send, f_recv, gains,
      pt_send, pt_recv, rb_send, line_rows, own_send, rows, s_send, s_recv, h_send, h_recv,
      y_send, y_recv,
-     info_a, info_az, info_b, info_by, info_c, info_cc,
+     info_a, info_az, info_b, info_by, info_cc,
      zs, zr, ys, yr, xs, xr, cs, cr, fs, fr, gs, gr) = refs[18:]
     z, y, c, x = (lax.axis_index(name) for name in ("z", "y", "c", "x"))
     nz, ny, nc, nx, b = d.nz, d.ny, d.nc, d.nx, d.b
@@ -153,9 +153,11 @@
     ]
     for copy in small:
         copy.start()
-    loads = [(key, kbuf), (val, vbuf), (down, dbuf)]
+    loads = [(key, kbuf), (val, vbuf)]
     for t in range(nx):
         loads += [(gate.at[:, t], gbuf.at[t]), (up.at[:, t], ubuf.at[t])]
+    for t in range(nx):
+        loads += [(down.at[:, pl.ds(t * d.xs, d.xs)], dbuf.at[t])]
     loads = [
         pltpu.make_async_copy(src, dst, load_sem.at[23 + i]) for i, (src, dst) in enumerate(loads)
     ]
@@ -204,11 +206,11 @@
     for t in range(nz):
         for j in range(nc):
             qa_send[t * nc + j] = moved[t * PAD : (t + 1) * PAD, j * share : (j + 1) * share]
-    lane = iota((8, d.nt), 1)
-    field = iota((8, d.nt), 0)
-    info = jnp.zeros((8, d.nt), F32)
+    lane = iota((4, 128), 1)
+    field = iota((4, 128), 0)
+    info = jnp.zeros((4, 128), F32)
     for r in range(b):
-        here = lane == slot * line + z * b + r
+        here = lane == z * b + r
         for j, number in enumerate((
             ids[0, r].astype(F32), ids[1, r].astype(F32), rw[0, r], rw[1, r],
         )):
@@ -237,6 +239,24 @@
         send(remote(info_a, info_az.at[z], zs.at[4 * nz + k], zr.at[4 * nz + k], z=up_z(k)))
         for k in far_first(nz)
     ]
+    for copy in qa_in:
+        copy.wait_recv()
+    own_a.wait()
+    own_q.wait()
+    rows_a = stacked(qa_recv, nz * nc)
+    part = d.ql // PAD
+    for copy in wq_in:
+        copy.wait_recv()
+    partial = dot(rows_a, wq_all[...])
+    fourth = (iota((nz * nc * PAD, 1), 0) & (PAD - 1)) == b
+    last = partial[:, b * part :]
+    for r in range(b):
+        span = slice(r * part, (r + 1) * part)
+        packed = jnp.where(fourth, pltpu.roll(last, b - r, 0), partial[:, span]).astype(BF16)
+        for t in range(nz * nc):
+            qp_send[t, :, span] = packed[t * PAD : (t + 1) * PAD]
+    qp_in = zc_exchange(2 * nz, qp_send, qp_recv)
+    own_p = keep(9, qp_send.at[me], qp_recv.at[me])
     wo_in = {
         k: send(remote(wo, wo_all.at[pl.ds(own_piece, d.rp)], ys.at[ny + k], yr.at[ny + k], y=up_y(k)))
         for k in far_first(ny)
@@ -249,59 +269,45 @@
     ]
     own_t = keep(8, ta_send.at[z], ta_recv.at[z])
 
-    for copy in qa_in:
-        copy.wait_recv()
-    own_a.wait()
-    own_q.wait()
-    rows_a = stacked(qa_recv, nz * nc)
-    for copy in wq_in:
-        copy.wait_recv()
-    partial = dot(rows_a, wq_all[...]).astype(BF16)
-    for t in range(nz * nc):
-        qp_send[t] = partial[t * PAD : (t + 1) * PAD]
-    qp_in = zc_exchange(2 * nz, qp_send, qp_recv)
-    own_p = keep(9, qp_send.at[me], qp_recv.at[me])
+    for copy in info_in:
+        copy.wait_recv()
+    info = info_a[...]
+    for k in range(1, nz):
+        info = info + info_az[up_z(k)]
+    info_by[y] = info
+    info_b[...] = info
+    info_y_in = [
+        send(remote(info_b, info_by.at[y], ys.at[2 * ny + k], yr.at[2 * ny + k], y=up_y(k)))
+        for k in far_first(ny)
+    ]
+    loads[0].wait()
+    loads[1].wait()
+
+    for copy in qp_in:
+        copy.wait_recv()
+    own_p.wait()
+    q = qp_recv[0].astype(F32)
+    for t in range(1, nz * nc):
+        q = q + qp_recv[t].astype(F32)
+    last = [q[b : b + 1, r * part : (r + 1) * part] for r in range(b)]
+    last = jnp.concatenate(last + [jnp.zeros((PAD - b, part), F32)], axis=0)
+    q = jnp.concatenate([q, last], axis=1)
+    mixed = attention(d, q, kbuf, vbuf, lens, hoff)
+    mx_send[...] = mixed
+    mx_in = [
+        send(remote(mx_send, mx_recv.at[z], zs.at[6 * nz + k], zr.at[6 * nz + k], z=up_z(k)))
+        for k in far_first(nz)
+    ]
+    own_m = keep(10, mx_send, mx_recv.at[z])
+
+    for copy in info_y_in:
+        copy.wait_recv()
+    info_c_in = send(remote(info_by, info_cc, cs.at[ny], cr.at[ny], c=other))
 
     for k in near_first(ny):
         wo_in[k].wait_recv()
         part = wo_all.at[pl.ds(pl.multiple_of((from_y(k) * nc + c) * d.rp, 8), d.rp)]
         wo_fwd.append(send(remote(part, part, cs.at[k], cr.at[k], c=other)))
-    for copy in info_in:
-        copy.wait_recv()
-    info = info_a[...]
-    for k in range(1, nz):
-        info = info + info_az[up_z(k)]
-    info_b[...] = info
-    info_y_in = [
-        send(remote(info_b, info_by.at[y], ys.at[2 * ny + k], yr.at[2 * ny + k], y=up_y(k)))
-        for k in far_first(ny)
-    ]
-    loads[0].wait()
-    loads[1].wait()
-
-    for copy in qp_in:
-        copy.wait_recv()
-    own_p.wait()
-    q = qp_recv[0].astype(F32)
-    for t in range(1, nz * nc):
-        q = q + qp_recv[t].astype(F32)
-    q = jnp.concatenate([q, jnp.zeros((8 - PAD, d.ql), F32)], axis=0)
-    mixed = attention(d, q, kbuf, vbuf, lens, hoff)
-    mx_send[...] = mixed[0:PAD]
-    mx_in = [
-        send(remote(mx_send, mx_recv.at[z], zs.at[6 * nz + k], zr.at[6 * nz + k], z=up_z(k)))
-        for k in far_first(nz)
-    ]
-    own_m = keep(10, mx_send, mx_recv.at[z])
-
-    for copy in info_y_in:
-        copy.wait_recv()
-    info = info_b[...]
-    for k in range(1, ny):
-        info = info + info_by[up_y(k)]
-    info_c[...] = info
-    info_c_in = send(remote(info_c, info_cc, cs.at[ny], cr.at[ny], c=other))
-
     pick_t = iota((line, nz * PAD), 0)
     pick_s = iota((line, nz * PAD), 1)
     within = pick_s & (PAD - 1)
@@ -310,9 +316,8 @@
         copy.wait_recv()
     own_t.wait()
     tok = dot(pick, stacked(ta_recv, nz))
-    own_token = onehot(iota((d.nt, line), 0) == iota((d.nt, line), 1) + slot * line)
     count = float(ny * nc)
-    own_ids = dot(info_b[...].astype(BF16), own_token)[0:1]
+    own_ids = info_b[...][0:1, :line]
     zone = iota((8, line), 0).astype(F32) * count
     bound = onehot((own_ids >= zone) & (own_ids < zone + count))
     bound_rank = dot(bound, onehot(iota((line, line), 0) < iota((line, line), 1)))
@@ -369,7 +374,11 @@
         away.start()
 
     info_c_in.wait_recv()
-    info = info_c[...] + info_cc[...]
+    near = [info_by[t] for t in range(ny)]
+    far = [info_cc[t] for t in range(ny)]
+    info = jnp.concatenate(
+        [jnp.where(c == 0, u, v)[:, :line] for u, v in zip(near, far)]
+        + [jnp.where(c == 0, v, u)[:, :line] for u, v in zip(near, far)], axis=1)
     info_out[...] = info
     id0 = info[0:1]
     id1 = info[1:2]
@@ -412,7 +421,8 @@
     owner_s = iota((ny * nz * PAD, d.nt), 0)
     owner_t = iota((ny * nz * PAD, d.nt), 1) - c * half_width
     r_of = owner_s & (PAD - 1)
-    first_of = (owner_s >> (PAD.bit_length() - 1)) * b
+    owner_i = owner_s >> (PAD.bit_length() - 1)
+    first_of = (owner_i & (ny - 1)) * line + (owner_i >> (ny.bit_length() - 1)) * b
     owners = onehot((r_of < b) & (first_of + r_of == owner_t))
     owners = dot(owners, chosen_tokens, ((1,), (1,)))
     homes = []
@@ -482,31 +492,37 @@
     own_s = keep(5, s_send.at[c], s_recv.at[x, our_slots])
     for copy in loads[2:]:
         copy.wait()
-    own_s.wait()
-    for copy in s_in:
-        copy.wait_recv()
-    wide = [s_recv[t].astype(F32) for t in range(nx)]
-    square = sum(jnp.sum(part * part, axis=1, keepdims=True) for part in wide)
-    scale = lax.rsqrt(square / d.width + 1e-06)
     gated = jnp.zeros((nc * SLOTS, d.ff), F32)
     upward = jnp.zeros((nc * SLOTS, d.ff), F32)
-    for t in range(nx):
-        part = (wide[t] * scale * gains[t]).astype(BF16)
+    square = jnp.zeros((nc * SLOTS, 1), F32)
+    waiting = dict(zip(xc, s_in))
+    own_s.wait()
+    for k in [0] + near_first(nx):
+        for j in range(nc):
+            if k or j:
+                waiting[(k, j)].wait_recv()
+        t = lax.rem(x - k + nx, nx)
+        part = s_recv[t].astype(F32)
+        square = square + jnp.sum(part * part, axis=1, keepdims=True)
+        part = (part * gains[t]).astype(BF16)
         gated = gated + dot(part, gbuf[t].reshape(d.xs, d.ff))
         upward = upward + dot(part, ubuf[t].reshape(d.xs, d.ff))
-    hidden = (gated / (1.0 + jnp.exp(-gated)) * upward).astype(BF16)
-    for t in range(nx):
-        h_send[t] = dot(hidden, dbuf[:, t * d.xs : (t + 1) * d.xs]).astype(BF16)
+    scale = lax.rsqrt(square / d.width + 1e-06)
+    gated = gated * scale
+    hidden = (gated / (1.0 + jnp.exp(-gated)) * (upward * scale)).astype(BF16)
 
     def to_half(j):
         return pl.ds(pl.multiple_of(up_c(j) * SLOTS, SLOTS), SLOTS)
 
-    h_in = [
-        send(remote(
-            h_send.at[up_x(k), to_half(j)], h_recv.at[x, our_slots],
-            xs.at[1 + nx * nc + k * nc + j], xr.at[nx + nx * nc + k * nc + j], x=up_x(k), c=up_c(j)))
-        for k, j in xc
-    ]
+    h_in = []
+    for k in far_first(nx) + [0]:
+        h_send[up_x(k)] = dot(hidden, dbuf[up_x(k)]).astype(BF16)
+        for j in range(nc):
+            if k or j:
+                h_in.append(send(remote(
+                    h_send.at[up_x(k), to_half(j)], h_recv.at[x, our_slots],
+                    xs.at[1 + nx * nc + k * nc + j], xr.at[nx + nx * nc + k * nc + j],
+                    x=up_x(k), c=up_c(j))))
     own_h = keep(6, h_send.at[x, our_slots], h_recv.at[x, our_slots])
     own_h.wait()
     for copy in h_in:
@@ -516,26 +532,33 @@
         total = total + h_recv[t].astype(F32)
     answer = total.astype(BF16).astype(F32) * slot_route
     part = d.xs // PAD
-    for r in range(b):
-        both = jnp.concatenate([answer[:, r * part : (r + 1) * part], answer[:, b * part :]], axis=0)
-        y_send[:, :, r * part : (r + 1) * part] = (
-            dot(homes[r], both.astype(BF16)).reshape(ny * nz, PAD, part).astype(BF16))
+    pairs = [
+        jnp.concatenate([answer[:, r * part : (r + 1) * part], answer[:, b * part :]], axis=0).astype(BF16)
+        for r in range(b)
+    ]
 
     def give(t, k):
         return remote(
-            y_send.at[up_y(k) * nz + t], y_recv.at[y * nz + z],
+            y_send.at[t * ny + up_y(k)], y_recv.at[y * nz + z],
             gs.at[t * ny + k], gr.at[z * ny + k], z=t, y=up_y(k))
 
-    for t in range(nz):
-        for k in far_first(ny):
-            send(give(t, k))
-
-        @pl.when(z != t)
-        def _():
-            give(t, 0).start()
+    some = nz // 2
+    for first_z in range(0, nz, some):
+        area = slice(first_z * ny, (first_z + some) * ny)
+        for r in range(b):
+            from_home = homes[r][area.start * PAD : area.stop * PAD]
+            y_send[area, :, r * part : (r + 1) * part] = (
+                dot(from_home, pairs[r]).reshape(some * ny, PAD, part).astype(BF16))
+        for t in range(first_z, first_z + some):
+            for k in far_first(ny):
+                send(give(t, k))
+
+            @pl.when(z != t)
+            def _():
+                give(t, 0).start()
 
     given = nz * (ny - 1)
-    own_y = keep(7, y_send.at[y * nz + z], y_recv.at[y * nz + z])
+    own_y = keep(7, y_send.at[z * ny + y], y_recv.at[y * nz + z])
     for j in range(d.nb):
         source = x * d.nb + j
 
@@ -604,8 +627,8 @@
         out_shape=(
             pltpu.VMEM((d.b, d.xs), BF16),
             jax.ShapeDtypeStruct((line, d.xs), BF16),
-            jax.ShapeDtypeStruct((8, d.nt), F32),
-            jax.ShapeDtypeStruct((1,), jnp.int32),
+            pltpu.VMEM((4, d.nt), F32),
+            pltpu.SMEM((1,), jnp.int32),
         ),
         in_specs=[outside] * 14,
         out_specs=(inside, outside, inside, pl.BlockSpec(memory_space=pltpu.SMEM)),
@@ -615,12 +638,12 @@
             pltpu.SMEM((d.b,), jnp.int32), pltpu.SMEM((d.ql // d.hd,), F32),
             pltpu.SMEM((2, d.b), jnp.int32), pltpu.SMEM((2, d.b), F32),
             vmem(d.b, d.cache, d.hd), vmem(d.b, d.cache, d.hd),
-            vmem(d.nx, d.nz, d.zb // d.nx, d.ff), vmem(d.nx, d.nz, d.zb // d.nx, d.ff), vmem(d.ff, d.width),
-            dma((26 + 2 * d.nx,)),
+            vmem(d.nx, d.nz, d.zb // d.nx, d.ff), vmem(d.nx, d.nz, d.zb // d.nx, d.ff), vmem(d.nx, d.ff, d.xs),
+            dma((25 + 3 * d.nx,)),
             vmem(d.nz, PAD, d.zb), vmem(d.nz, PAD, d.zb),
             vmem(d.nz * d.nc, PAD, d.zb // d.nc), vmem(d.nz * d.nc, PAD, d.zb // d.nc),
             vmem(d.ny * d.rp, d.ql), vmem(d.zb, d.ql),
-            vmem(d.nz * d.nc, PAD, d.ql), vmem(d.nz * d.nc, PAD, d.ql),
+            vmem(d.nz * d.nc, PAD, d.ql // PAD * d.b), vmem(d.nz * d.nc, PAD, d.ql // PAD * d.b),
             vmem(PAD, d.ql), vmem(d.nz, PAD, d.ql),
             vmem(d.nx, d.nz, SLOTS // 2, 128), vmem(d.nz, SLOTS // 2, 128),
             vmem(d.nx, d.nz, SLOTS // 2, 128), vmem(d.nx, d.nz, SLOTS // 2, 128),
@@ -630,9 +653,8 @@
             vmem(d.nc, SLOTS, d.xs), vmem(d.nx, d.nc * SLOTS, d.xs),
             vmem(d.nx, d.nc * SLOTS, d.xs), vmem(d.nx, d.nc * SLOTS, d.xs),
             vmem(d.ny * d.nz, PAD, d.xs // PAD * d.b), vmem(d.ny * d.nz, PAD, d.xs // PAD * d.b),
-            vmem(8, d.nt, dtype=F32), vmem(d.nz, 8, d.nt, dtype=F32),
-            vmem(8, d.nt, dtype=F32), vmem(d.ny, 8, d.nt, dtype=F32),
-            vmem(8, d.nt, dtype=F32), vmem(8, d.nt, dtype=F32),
+            vmem(4, 128, dtype=F32), vmem(d.nz, 4, 128, dtype=F32), vmem(4, 128, dtype=F32),
+            vmem(d.ny, 4, 128, dtype=F32), vmem(d.ny, 4, 128, dtype=F32),
             dma((10 * d.nz,)), dma((10 * d.nz,)),
             dma((5 * d.ny,)), dma((5 * d.ny,)),
             dma((1 + 2 * d.nx * d.nc,)), dma((d.nx + 2 * d.nx * d.nc,)),

time: 65.7 us -> 63.4 us (0.965)
  Pallas kernels: 64.3 us -> 62.6 us
    pallas_call x1, Pallas kernels: 64.3 us -> 62.6 us  [layer(): pl.pallas_call(functools.partial(kernel, d), out_shape=(pltpu.VMEM((d.b,...]
where the time goes in v2:
time: 63.4 us; the launch traced here: 63.2 us
  Pallas kernels  62.6 us (99%)
    pallas_call x1, Pallas kernels, layer(): pl.pallas_call(functools.partial(kernel, d), out_shape=(pltpu.VMEM((d.b,...  62.6 us

profile of v2, /device:TPU:1, one launch (start us, length us, event | category | flops | bytes accessed | tf_op | source)
XLA Modules:
  0.0 63.2 jit_solution(12056558589532842892)
XLA Ops:
  0.0 0.0 copy-start.1
  0.0 62.6 %shard_map.138 = (bf16[3,512]{1,0:T(4,128)(2,1)S(1)}, bf16[24,512]{1,0:T(8,128)(2,1)S(1)}, f32[4,384]{1,0:T(4,128)S(1)}, s32[1]{0:T(128)S(4)}) custom-call(bf16[3,2048]{1,0:T(4,128)(2,1)} %refs_0_.1, f32[1,2048]{1,0:T(1,128)} %bitcast.49, bf16[16,512]{1,0:T(8,128)(2,1)} %refs_2_.1, bf16[3,1024,128]{2,1,0:T(8,128)(2,1)} %bitcast.45, ...), custom_call_target="tpu_custom_call" | custom-call | tf_op jit(solution)/shard_map/pallas_call | solution.py:625
  62.6 0.0 copy-done.1
  62.6 0.6 copy.35
  (1 shorter events, 0.0 us)
Async XLA Ops:
  0.0 62.6 %copy-start.1 = (f32[2048]{0:T(1024)S(1)}, f32[2048]{0:T(1024)}, u32[]{:S(2)}) copy-start(f32[2048]{0:T(1024)} %param.24) | copy-start | bytes 24580

commit v3 on v2

--- a/solution.py
+++ b/solution.py
@@ -283,12 +283,11 @@
     loads[0].wait()
     loads[1].wait()
 
-    for copy in qp_in:
-        copy.wait_recv()
     own_p.wait()
-    q = qp_recv[0].astype(F32)
-    for t in range(1, nz * nc):
-        q = q + qp_recv[t].astype(F32)
+    q = qp_recv[me].astype(F32)
+    for (k, j), copy in zip(zc, qp_in):
+        copy.wait_recv()
+        q = q + qp_recv[lax.rem(z - k + nz, nz) * nc + lax.rem(c - j + nc, nc)].astype(F32)
     last = [q[b : b + 1, r * part : (r + 1) * part] for r in range(b)]
     last = jnp.concatenate(last + [jnp.zeros((PAD - b, part), F32)], axis=0)
     q = jnp.concatenate([q, last], axis=1)
@@ -589,6 +588,7 @@
     for copy in pending[:-given]:
         copy.wait_send()
     own_y.wait()
+    total = jnp.zeros((PAD, part * b), F32)
     for t in range(nz):
         for k in near_first(ny):
             remote(
@@ -599,10 +599,11 @@
         def _():
             remote(
                 y_send.at[0], y_recv.at[y * nz + t], gs.at[0], gr.at[t * ny], z=t).wait_recv()
-
-    total = y_recv[0].astype(F32)
-    for t in range(1, ny * nz):
-        total = total + y_recv[t].astype(F32)
+        arrived = [y_recv[u * nz + t].astype(F32) for u in range(ny)]
+        while len(arrived) > 1:
+            arrived = [sum(arrived[u : u + 2]) for u in range(0, len(arrived), 2)]
+        total = total + arrived[0]
+
     last = jnp.concatenate([total[b : b + 1, r * part : (r + 1) * part] for r in range(b)], axis=0)
     out[...] = (resid[0:b] + jnp.concatenate([total[0:b], last], axis=1)).astype(BF16)
     for t in range(nz):

time: 63.4 us -> 63.5 us (level)
  no operation moved by 1% of the time
where the time goes in v3:
time: 63.5 us; the launch traced here: 63.3 us
  Pallas kernels  62.7 us (99%)
    pallas_call x1, Pallas kernels, layer(): pl.pallas_call(functools.partial(kernel, d), out_shape=(pltpu.VMEM((d.b,...  62.7 us

profile of v3, /device:TPU:1, one launch (start us, length us, event | category | flops | bytes accessed | tf_op | source)
XLA Modules:
  0.0 63.3 jit_solution(5392949074771247764)
XLA Ops:
  0.0 0.0 copy-start.1
  0.0 62.7 %shard_map.138 = (bf16[3,512]{1,0:T(4,128)(2,1)S(1)}, bf16[24,512]{1,0:T(8,128)(2,1)S(1)}, f32[4,384]{1,0:T(4,128)S(1)}, s32[1]{0:T(128)S(4)}) custom-call(bf16[3,2048]{1,0:T(4,128)(2,1)} %refs_0_.1, f32[1,2048]{1,0:T(1,128)} %bitcast.49, bf16[16,512]{1,0:T(8,128)(2,1)} %refs_2_.1, bf16[3,1024,128]{2,1,0:T(8,128)(2,1)} %bitcast.45, ...), custom_call_target="tpu_custom_call" | custom-call | tf_op jit(solution)/shard_map/pallas_call | solution.py:626
  62.7 0.0 copy-done.1
  62.7 0.6 copy.35
  (1 shorter events, 0.0 us)
Async XLA Ops:
  0.0 62.7 %copy-start.1 = (f32[2048]{0:T(1024)S(1)}, f32[2048]{0:T(1024)}, u32[]{:S(2)}) copy-start(f32[2048]{0:T(1024)} %param.24) | copy-start | bytes 24580
